TPU v7x, 32 devices: a whole 2x2x4 slice. The times are simulated.
32 devices in a mesh: grp: 2 (over y), fs: 4 (over z), tp: 4 (over x, core).
Axes of the slice: x: 2, y: 2, z: 4, core: 2. Of those that a mesh axis runs over, the one named last changes fastest.
Arguments:
- tokens: bfloat16 [4096, 2048], P(('grp', 'fs')), parts along dimension 0, may hold values from -6 to 6
- pre_gain: float32 [2048], replicated, may hold values from 0.1 to 1.9
- up_weight: float32 [2048, 8192], P('fs', 'tp'), may hold values from -0.125 to 0.125
- up_scale: float32 [8192], P('tp'), may hold values from 0.3 to 3
- down_weight: float32 [8192, 2048], P('tp', 'fs'), may hold values from -0.0625 to 0.0625
- down_scale: float32 [2048], P('fs'), may hold values from 0.3 to 3
- post_gain: float32 [2048], replicated, may hold values from 0.1 to 1.9
Outputs:
- mixed: bfloat16 [4096, 2048], P(('grp', 'fs')), parts along dimension 0
There are 2 independent parts, one for each index of `grp`. A program takes and returns all parts, laid end to end along the dimension named above; an argument that names none is the same for every part. Nothing has to cross between parts.
All inputs are finite; a program needn't handle non-finite values.
Results may differ from a plain program's by a relative error of at most 0.01.
Values may be sent and summed in bfloat16 or wider, within the bound.
A program may use at most 64 MiB of HBM per device.

v0:
```python
import functools

import jax
import jax.numpy as jnp
from jax import lax
from jax.experimental import pallas as pl
from jax.experimental.pallas import tpu as pltpu
from jax.sharding import PartitionSpec as P

epsilon = 1e-06
MESH = pl.DeviceIdType.MESH
CHUNKS = 2


def rms_rows(values, scaling):
    return values * lax.rsqrt(jnp.mean(values * values, axis=-1, keepdims=True) + epsilon) * scaling


def activate(lifted, up_scale):
    return jnp.square(jax.nn.relu(lifted * up_scale)).astype(jnp.bfloat16)


def plain(tokens, pre_gain, up_weight, up_scale, down_weight, down_scale, post_gain):
    residual = tokens.astype(jnp.float32)
    normed = rms_rows(residual, pre_gain).astype(jnp.bfloat16)
    up_cast = up_weight.astype(jnp.bfloat16)
    down_cast = down_weight.astype(jnp.bfloat16)
    column_scales = lax.all_gather(down_scale, "fs", axis=0, tiled=True)
    up_full, down_full = (
        lax.all_gather(up_cast, "fs", axis=0, tiled=True),
        lax.all_gather(down_cast, "fs", axis=1, tiled=True),
    )
    lifted = jnp.dot(normed, up_full, preferred_element_type=jnp.float32)
    hidden = activate(lifted, up_scale)
    partials = jnp.dot(hidden, down_full, preferred_element_type=jnp.float32)
    partials = (partials * column_scales).astype(jnp.bfloat16)
    summed = lax.psum(partials, "tp").astype(jnp.float32)
    branch = lax.optimization_barrier(summed.astype(jnp.bfloat16)).astype(jnp.float32)
    return (residual + rms_rows(branch, post_gain)).astype(jnp.bfloat16)


def kernel(nc, tokens, up_in, down_in, up_scale, down_scale, pre_gain, post_gain, out, res, up_f32, down_f32, up,
           down, tok, hid, scl, keep, core_out, core_in,
           x_out, x_in, branch, ship, send, wrecv, tok_recv, scl_recv, core_recv, x_recv, br_recv, local, one_sem):
    g, z, t = lax.axis_index("grp"), lax.axis_index("fs"), lax.axis_index("tp")
    core, x = lax.rem(t, 2), t // 2
    pair = z // 2
    outer, inner, other = 3 * pair, 1 + pair, 2 - pair
    outer2 = 3 - outer
    is_outer = z == outer
    n_tp = 4
    rows = tokens.shape[0]
    depth, half = up_in.shape[0], up_in.shape[1] // 2
    du, dc = depth // nc, depth // nc
    quarter = rows // n_tp
    core_peer, x_peer = x * 2 + 1 - core, (1 - x) * 2 + core

    def at_half(h):
        return pl.ds(pl.multiple_of(h * half, half), half)

    def load(kind, c, h):
        if kind == 0:
            place = pl.ds(c * du, du), at_half(h)
            pair = up_in.at[place], up_f32.at[place]
        else:
            place = at_half(h), pl.ds(c * dc, dc)
            pair = down_in.at[place], down_f32.at[place]
        return pltpu.make_async_copy(*pair, local.at[kind, c, h])

    for c in range(nc):
        load(0, c, g).start()
    fetch = pltpu.make_async_copy(tokens, res, one_sem.at[0])
    fetch.start()
    for c in range(nc):
        load(0, c, 1 - g).start()
    for h in (g, 1 - g):
        for c in range(nc):
            load(1, c, h).start()

    barrier = pltpu.get_barrier_semaphore()
    peers = [{"fs": lax.rem(z + o, 4)} for o in range(1, 4)] + [{"grp": 1 - g}]
    peers += [{"tp": lax.rem(t + o, n_tp)} for o in range(1, n_tp)]
    for peer in peers:
        pl.semaphore_signal(barrier, inc=1, device_id=peer, device_id_type=MESH)
    pl.semaphore_wait(barrier, len(peers))

    def remote(src, dst, s, r, peer):
        return pltpu.make_async_remote_copy(src_ref=src, dst_ref=dst, send_sem=send.at[s], recv_sem=r,
                                            device_id=peer, device_id_type=MESH)

    def up_slot(zz, c, h):
        return up.at[h, pl.ds(pl.multiple_of(zz * depth + c * du, du), du), :]

    def down_slot(zz, c, h):
        return down.at[zz * nc + c, pl.ds(pl.multiple_of(h * half, half), half), :]

    slots = (up_slot, down_slot)

    def cast(kind, c, h):
        load(kind, c, h).wait()
        if kind == 0:
            up[h, pl.ds(pl.multiple_of(z * depth + c * du, du), du), :] = up_f32[
                pl.ds(c * du, du), at_half(h)].astype(jnp.bfloat16)
        else:
            down[z * nc + c, at_half(h), :] = down_f32[at_half(h), pl.ds(c * dc, dc)].astype(jnp.bfloat16)

    def norm_rows(first, n, step):
        def one(i, _):
            part = pl.ds(pl.multiple_of(first + i * step, step), step)
            tok[part, :] = rms_rows(res[part, :].astype(jnp.float32), pre_gain[...]).astype(jnp.bfloat16)
            return 0
        lax.fori_loop(0, n // step, one, 0)

    def tok_slot(n, q):
        return tok.at[pl.ds(pl.multiple_of(n * rows + q * quarter, quarter), quarter), :]

    def weight(kind, src, zz, c, h, s, peer):
        return remote(src, slots[kind](zz, c, h), s, wrecv.at[kind, zz, c, h], peer)

    def arrived(kind, zz, c, h):
        slot = slots[kind](zz, c, h)
        weight(kind, slot, zz, c, h, 0, {"fs": z}).wait_recv()

    def block(b):
        return branch.at[b]

    @pl.when(is_outer)
    def _():
        started = []
        to = {"fs": inner}

        def go(copy):
            copy.start()
            started.append(copy)

        go(remote(down_scale, scl.at[z], 0, scl_recv.at[z], to))
        go(remote(down_scale, scl.at[z], 1, scl_recv.at[z], {"fs": other}))
        for c in range(nc):
            cast(0, c, g)
            go(weight(0, up_slot(z, c, g), z, c, g, 2 + c, to))
        fetch.wait()
        norm_rows(t * quarter, quarter, min(quarter, 64))
        go(remote(tok_slot(0, t), tok_slot(1, t), 2 + nc, tok_recv.at[t], to))
        for c in range(nc):
            cast(0, c, 1 - g)
            go(weight(0, up_slot(z, c, 1 - g), z, c, 1 - g, 3 + nc + c, to))
        for c in range(nc):
            cast(1, c, g)
            go(weight(1, down_slot(z, c, g), z, c, g, 3 + 2 * nc + c, to))
        for c in range(nc):
            cast(1, c, 1 - g)
            go(weight(1, down_slot(z, c, 1 - g), z, c, 1 - g, 3 + 3 * nc + c, to))
        for copy in started:
            copy.wait_send()
        for b in range(4 * nc):
            remote(block(b), block(b), 0, br_recv.at[b], to).wait_recv()

    @pl.when(jnp.logical_not(is_outer))
    def _():
        started = []
        counter = [0]

        def fresh():
            counter[0] += 1
            return counter[0] - 1

        def go(copy):
            copy.start()
            started.append(copy)

        across, beside = {"fs": other}, {"grp": 1 - g}
        for c in range(nc):
            cast(0, c, g)
            go(weight(0, up_slot(z, c, g), z, c, g, fresh(), across))
        go(remote(down_scale, scl.at[z], fresh(), scl_recv.at[z], across))
        own_scale = pltpu.make_async_copy(down_scale, scl.at[z], one_sem.at[1])
        own_scale.start()
        for c in range(nc):
            cast(1, c, g)
        fetch.wait()
        norm_rows(0, rows, 64)
        own_scale.wait()

        def forward(kind, c):
            arrived(kind, outer, c, g)
            go(weight(kind, slots[kind](outer, c, g), outer, c, g, fresh(), across))

        def relay(kind, zz, c):
            arrived(kind, zz, c, g)
            go(weight(kind, slots[kind](zz, c, g), zz, c, g, fresh(), beside))

        for c in range(nc):
            forward(0, c)
            relay(0, other, c)
        for c in range(nc):
            go(weight(1, down_slot(z, c, g), z, c, g, fresh(), across))
        remote(tok_slot(1, t), tok_slot(1, t), 0, tok_recv.at[t], {"fs": outer}).wait_recv()
        for o in range(1, n_tp):
            go(remote(tok_slot(1, t), tok_slot(1, t), fresh(), tok_recv.at[t], {"tp": lax.rem(t + o, n_tp)}))
        for c in range(nc):
            cast(0, c, 1 - g)
        for c in range(nc):
            cast(1, c, 1 - g)
        for c in range(nc):
            relay(0, outer2, c)
        for o in range(1, n_tp):
            q = lax.rem(t + o, n_tp)
            remote(tok_slot(1, q), tok_slot(1, q), 0, tok_recv.at[q], {"tp": q}).wait_recv()

        tile = dc

        def lift(h):
            def one(i, _):
                columns = pl.ds(pl.multiple_of(i * tile, tile), tile)
                whole = pl.ds(pl.multiple_of(h * half + i * tile, tile), tile)
                for n in range(2):
                    part = pl.ds(n * rows, rows)
                    lifted = jnp.dot(tok[part, :], up[h, :, columns], preferred_element_type=jnp.float32)
                    hid[part, whole] = activate(lifted, up_scale[:, whole])
                return 0
            lax.fori_loop(0, half // tile, one, 0)

        lift(g)
        relay(1, other, 0)
        for c in range(nc):
            arrived(0, outer, c, 1 - g)
            arrived(0, other, c, 1 - g)
            arrived(0, outer2, c, 1 - g)
        lift(1 - g)
        for c in range(1, nc):
            relay(1, other, c)

        def project(zz, c):
            b = zz * nc + c
            theirs = jnp.dot(hid[pl.ds(pl.multiple_of((1 - core) * rows, rows), rows), :], down[b],
                             preferred_element_type=jnp.float32)
            core_out[b] = theirs.astype(jnp.bfloat16)
            go(remote(core_out.at[b], core_in.at[b], fresh(), core_recv.at[b], {"tp": core_peer}))
            keep[lax.rem(b, 2)] = jnp.dot(hid[pl.ds(pl.multiple_of(core * rows, rows), rows), :], down[b],
                              preferred_element_type=jnp.float32)

        def cross(zz, c):
            b = zz * nc + c
            remote(core_out.at[b], core_in.at[b], 0, core_recv.at[b], {"tp": core_peer}).wait_recv()
            x_out[b] = (keep[lax.rem(b, 2)] + core_in[b].astype(jnp.float32)).astype(jnp.bfloat16)
            go(remote(x_out.at[b], x_in.at[b], fresh(), x_recv.at[b], {"tp": x_peer}))

        last = []
        for _ in range(4 * nc):
            last.append((fresh(), fresh()))

        def finish(i, zz, c):
            b = zz * nc + c
            remote(x_out.at[b], x_in.at[b], 0, x_recv.at[b], {"tp": x_peer}).wait_recv()
            total = x_out[b].astype(jnp.float32) + x_in[b].astype(jnp.float32)
            value = (total * scl[zz, :, pl.ds(c * dc, dc)]).astype(jnp.bfloat16)

            @pl.when(core == 0)
            def _():
                branch[b] = value
                remote(block(b), block(b), last[i][0], br_recv.at[b], {"tp": core_peer}).start()

            @pl.when(core == 1)
            def _():
                ship[b] = value
                for k in range(2):
                    remote(ship.at[b], block(b), last[i][k], br_recv.at[b], {"fs": outer, "tp": x * 2 + k}).start()

        for zz in (outer, other, outer2):
            remote(down_scale, scl.at[zz], 0, scl_recv.at[zz], {"fs": zz}).wait_recv()

        order = [(z, c) for c in range(nc)] + [(other, c) for c in range(nc)]
        for c in range(nc):
            order += [(outer2, c), (outer, c)]
        n = len(order)
        for i in range(n + 2):
            if i < n:
                zz, c = order[i]
                if i >= nc:
                    arrived(1, zz, c, 1 - g)
                project_now = True
            else:
                project_now = False
            if 0 <= i - 1 < n:
                cross(*order[i - 1])
            if project_now:
                project(*order[i])
            if 0 <= i - 2 < n:
                finish(i - 2, *order[i - 2])
            if i < nc:
                forward(1, i)
            elif i < 2 * nc:
                relay(1, outer2, i - nc)
        for copy in started:
            copy.wait_send()
        for i, (zz, c) in enumerate(order):
            b = zz * nc + c

            @pl.when(core == 0)
            def _():
                remote(block(b), block(b), last[i][0], br_recv.at[b], {"tp": core_peer}).wait_send()

            @pl.when(core == 1)
            def _():
                for k in range(2):
                    remote(ship.at[b], block(b), last[i][k], br_recv.at[b], {"fs": outer, "tp": x * 2 + k}).wait_send()
                remote(block(b), block(b), last[i][0], br_recv.at[b], {"tp": core_peer}).wait_recv()

    def close(i, _):
        part = pl.ds(pl.multiple_of(i * 64, 64), 64)
        row = jnp.concatenate([branch[b, part, :] for b in range(4 * nc)], axis=1).astype(jnp.float32)
        out[part, :] = (res[part, :].astype(jnp.float32) + rms_rows(row, post_gain[...])).astype(jnp.bfloat16)
        return 0

    lax.fori_loop(0, rows // 64, close, 0)


def fused(tokens, pre_gain, up_weight, up_scale, down_weight, down_scale, post_gain):
    nc = CHUNKS
    rows, width = tokens.shape
    depth, ff = up_weight.shape
    half, dc = ff // 2, depth // nc
    blocks = 4 * nc
    bf, f32 = jnp.bfloat16, jnp.float32
    dma = pltpu.SemaphoreType.DMA
    anywhere, vmem = pl.BlockSpec(memory_space=pl.ANY), pl.BlockSpec(memory_space=pltpu.VMEM)
    return pl.pallas_call(
        functools.partial(kernel, nc),
        out_shape=jax.ShapeDtypeStruct((rows, width), bf),
        in_specs=[anywhere, anywhere, anywhere, vmem, vmem, vmem, vmem],
        out_specs=vmem,
        scratch_shapes=[
            pltpu.VMEM((rows, width), bf),
            pltpu.VMEM((depth, ff), f32),
            pltpu.VMEM((ff, depth), f32),
            pltpu.VMEM((2, width, half), bf),
            pltpu.VMEM((blocks, ff, dc), bf),
            pltpu.VMEM((2 * rows, width), bf),
            pltpu.VMEM((2 * rows, ff), bf),
            pltpu.VMEM((4, 1, depth), f32),
            pltpu.VMEM((2, rows, dc), f32),
            pltpu.VMEM((blocks, rows, dc), bf),
            pltpu.VMEM((blocks, rows, dc), bf),
            pltpu.VMEM((blocks, rows, dc), bf),
            pltpu.VMEM((blocks, rows, dc), bf),
            pltpu.VMEM((blocks, rows, dc), bf),
            pltpu.VMEM((blocks, rows, dc), bf),
            dma((64 * nc,)),
            dma((2, 4, nc, 2)),
            dma((4,)),
            dma((4,)),
            dma((blocks,)),
            dma((blocks,)),
            dma((blocks,)),
            dma((2, nc, 2)),
            dma((2,)),
        ],
        compiler_params=pltpu.CompilerParams(
            collective_id=0, has_side_effects=True, vmem_limit_bytes=60 << 20
        ),
    )(tokens, up_weight, down_weight, up_scale.reshape(1, ff), down_scale.reshape(1, depth),
      pre_gain.reshape(1, width), post_gain.reshape(1, width))


def solution(mesh):
    placed = (P(("grp", "fs"), None), P(), P("fs", "tp"), P("tp"), P("tp", "fs"), P("fs"), P())
    sizes = mesh.shape
    line = sizes["grp"] == 2 and sizes["fs"] == 4 and sizes["tp"] == 4
    return jax.shard_map(
        fused if line else plain, mesh=mesh, in_specs=placed, out_specs=P(("grp", "fs"), None), check_vma=False
    )
```

profile of v0, /device:TPU:0, one launch (start us, length us, event | category | flops | bytes accessed | tf_op | source)
XLA Modules:
  0.0 147.8 jit_solution(11522018145990187460)
XLA Ops:
  0.0 144.6 %shard_map.73 = bf16[512,2048]{1,0:T(8,128)(2,1)} custom-call(bf16[512,2048]{1,0:T(8,128)(2,1)} %tokens.1, f32[512,2048]{1,0:T(8,128)} %up_in.1, f32[2048,512]{1,0:T(8,128)} %down_in.1, f32[1,2048]{1,0:T(1,128)} %bitcast.4, f32[1,512]{1,0:T(1,128)} %bitcast.7, f32[1,2048]{1,0:T(1,128)} %bitcast.5, f32[1,2048]{1,0:T(1,128)} %bitcast.6), custom_call_target="tpu_custom_call" | custom-call | tf_op jit(solution)/shard_map/pallas_call | solution.py:327
  144.6 3.2 %copy.9 = bf16[512,2048]{1,0:T(8,128)(2,1)} copy(bf16[512,2048]{1,0:T(8,128)(2,1)} %shard_map.73) | data formatting | bytes 4194304
where the time goes:
time: 150 us; the launch traced here: 148 us
  Pallas kernels  145 us (97%)
  local copies, waits for them, and re-layouts  3.16 us (2%)
    pallas_call x1, Pallas kernels, fused(): pl.pallas_call(functools.partial(kernel, nc), out_shape=jax.ShapeDtypeStr...  145 us
    unnamed x1, local copies, waits for them, and re-layouts  3.16 us

commit v1 on v0

v1 whole, which is shorter than its diff:
```python
import functools

import jax
import jax.numpy as jnp
from jax import lax
from jax.experimental import pallas as pl
from jax.experimental.pallas import tpu as pltpu
from jax.sharding import PartitionSpec as P

epsilon = 1e-06
MESH = pl.DeviceIdType.MESH
PIECES = 4
WIDTHS = ((2, 2), (2, 2), (2, 2), (2, 1, 1))


def rms_rows(values, scaling):
    return values * lax.rsqrt(jnp.mean(values * values, axis=-1, keepdims=True) + epsilon) * scaling


def activate(lifted, up_scale):
    return jnp.square(jax.nn.relu(lifted * up_scale)).astype(jnp.bfloat16)


def plain(tokens, pre_gain, up_weight, up_scale, down_weight, down_scale, post_gain):
    residual = tokens.astype(jnp.float32)
    normed = rms_rows(residual, pre_gain).astype(jnp.bfloat16)
    up_cast = up_weight.astype(jnp.bfloat16)
    down_cast = down_weight.astype(jnp.bfloat16)
    column_scales = lax.all_gather(down_scale, "fs", axis=0, tiled=True)
    up_full, down_full = (
        lax.all_gather(up_cast, "fs", axis=0, tiled=True),
        lax.all_gather(down_cast, "fs", axis=1, tiled=True),
    )
    lifted = jnp.dot(normed, up_full, preferred_element_type=jnp.float32)
    hidden = activate(lifted, up_scale)
    partials = jnp.dot(hidden, down_full, preferred_element_type=jnp.float32)
    partials = (partials * column_scales).astype(jnp.bfloat16)
    summed = lax.psum(partials, "tp").astype(jnp.float32)
    branch = lax.optimization_barrier(summed.astype(jnp.bfloat16)).astype(jnp.float32)
    return (residual + rms_rows(branch, post_gain)).astype(jnp.bfloat16)


def kernel(tokens, up_in, down_in, up_scale, down_scale, pre_gain, post_gain, out, res, up_f32, down_f32, up, down,
           tok, acc, hid, scl, keep, core_out, core_in, y_out, y_in, xz_out, x_in, branch, send, up_recv, down_recv,
           tok_recv, scl_recv, core_recv, y_recv, x_recv, br_recv, local, one_sem, out_sem):
    g, z, t = lax.axis_index("grp"), lax.axis_index("fs"), lax.axis_index("tp")
    core, x = lax.rem(t, 2), t // 2
    pair = z // 2
    outer, inner, other = 3 * pair, 1 + pair, 2 - pair
    outer2 = 3 - outer
    is_outer = z == outer
    n_tp, np_ = 4, PIECES
    rows, width = tokens.shape
    depth, half = up_in.shape[0], up_in.shape[1] // 2
    du, dc, quarter = depth // np_, depth // np_, rows // np_
    core_peer, x_peer, cross_peer = x * 2 + 1 - core, (1 - x) * 2 + core, (1 - x) * 2 + 1 - core
    bf, f32 = jnp.bfloat16, jnp.float32

    def at(i, size):
        return pl.ds(pl.multiple_of(i * size, size), size)

    def load(kind, c):
        if kind == 0:
            copy = up_in.at[pl.ds(c * du, du), at(g, half)], up_f32.at[pl.ds(c * du, du), :]
        else:
            copy = down_in.at[at(g, half), pl.ds(c * dc, dc)], down_f32.at[:, pl.ds(c * dc, dc)]
        return pltpu.make_async_copy(*copy, local.at[kind, c])

    load(0, 0).start()
    fetch = pltpu.make_async_copy(tokens, res, one_sem.at[0])
    fetch.start()
    for c in range(1, np_):
        load(0, c).start()
    for c in range(np_):
        load(1, c).start()

    barrier = pltpu.get_barrier_semaphore()
    peers = [{"fs": lax.rem(z + o, 4)} for o in range(1, 4)] + [{"grp": 1 - g}]
    peers += [{"tp": lax.rem(t + o, n_tp)} for o in range(1, n_tp)]
    for peer in peers:
        pl.semaphore_signal(barrier, inc=1, device_id=peer, device_id_type=MESH)
    pl.semaphore_wait(barrier, len(peers))

    def remote(src, dst, s, r, peer):
        return pltpu.make_async_remote_copy(src_ref=src, dst_ref=dst, send_sem=send.at[s], recv_sem=r,
                                            device_id=peer, device_id_type=MESH)

    def same(ref, s, r, peer):
        return remote(ref, ref, s, r, peer)

    def slot(kind, zz, c):
        if kind == 0:
            return up.at[at(zz * np_ + c, du), :], up_recv.at[zz, c]
        return down.at[zz * np_ + c], down_recv.at[zz, c]

    def cast(kind, c):
        load(kind, c).wait()
        if kind == 0:
            up[at(z * np_ + c, du), :] = up_f32[pl.ds(c * du, du), :].astype(bf)
        else:
            down[z * np_ + c] = down_f32[:, pl.ds(c * dc, dc)].astype(bf)

    def weight(kind, zz, c, s, peer):
        ref, r = slot(kind, zz, c)
        return same(ref, s, r, peer)

    def arrived(kind, zz, c):
        weight(kind, zz, c, 0, {"fs": other}).wait_recv()

    def piece(gg, kind, k):
        b = kind * 2 + gg
        return tok.at[at(b * np_ + k, quarter), :], tok_recv.at[b, k]

    def pass_tok(gg, kind, k, s, peer):
        ref, r = piece(gg, kind, k)
        return same(ref, s, r, peer)

    def have_tok(gg, kind, k):
        pass_tok(gg, kind, k, 0, {"fs": other}).wait_recv()

    def norm(b, k):
        def one(i, _):
            source = pl.ds(pl.multiple_of(k * quarter + i * 64, 64), 64)
            target = pl.ds(pl.multiple_of((b * np_ + k) * quarter + i * 64, 64), 64)
            tok[target, :] = rms_rows(res[source, :].astype(f32), pre_gain[...]).astype(bf)
            return 0
        lax.fori_loop(0, quarter // 64, one, 0)

    blocks = (inner, outer, other, outer2)
    units = []
    for j, widths in enumerate(WIDTHS):
        k = 0
        for w in widths:
            units.append((blocks[j], k, w, j))
            k += w
    n = len(units)

    def part(ref, i):
        zz, k, w, _ = units[i]
        return ref.at[pl.ds(zz * np_ + k, w)]

    started = []
    counter = [0]

    def fresh():
        counter[0] += 1
        return counter[0] - 1

    def go(copy):
        copy.start()
        started.append(copy)

    last = [fresh() for _ in range(n)]

    def value(i, first, second):
        zz, k, w, _ = units[i]
        for j in range(w):
            b = zz * np_ + k + j
            total = first[b].astype(f32) + second[b].astype(f32)
            branch[b] = (total * scl[zz, :, pl.ds((k + j) * dc, dc)]).astype(bf)

    def share(i):
        return same(part(branch, i), last[i], br_recv.at[i], {"tp": core_peer})

    for o in range(1, 4):
        go(remote(down_scale, scl.at[z], fresh(), scl_recv.at[z], {"fs": lax.rem(z + o, 4)}))
    own_scale = pltpu.make_async_copy(down_scale, scl.at[z], one_sem.at[1])
    own_scale.start()

    def scales():
        own_scale.wait()
        for o in range(1, 4):
            zz = lax.rem(z + o, 4)
            remote(down_scale, scl.at[zz], 0, scl_recv.at[zz], {"fs": zz}).wait_recv()

    @pl.when(is_outer)
    def _():
        mark = len(started)
        to = {"fs": inner}
        fetch.wait()
        norm(2 + g, t)
        go(pass_tok(g, 1, t, fresh(), to))
        for kind in range(2):
            for c in range(np_):
                cast(kind, c)
                go(weight(kind, z, c, fresh(), to))
        scales()

        @pl.when(core == 1)
        def _():
            relays = [fresh() for _ in range(n)]

            def relay(i):
                return remote(part(x_in, i), part(y_in, i), relays[i], y_recv.at[i], {"tp": x_peer})

            for i in range(n + 1):
                if i < n:
                    remote(part(x_in, i), part(x_in, i), 0, x_recv.at[i], {"fs": inner}).wait_recv()
                    relay(i).start()
                if i >= 1:
                    relay(i - 1).wait_recv()
                    value(i - 1, x_in, y_in)
                    share(i - 1).start()
            for i in range(n):
                relay(i).wait_send()
                share(i).wait_send()

        @pl.when(core == 0)
        def _():
            for i in range(n):
                share(i).wait_recv()

        for copy in started[mark:]:
            copy.wait_send()
        del started[mark:]

    @pl.when(jnp.logical_not(is_outer))
    def _():
        mark = len(started)
        across, beside, next_core = {"fs": other}, {"grp": 1 - g}, {"tp": core_peer}
        for c in range(np_):
            cast(0, c)
            go(weight(0, z, c, fresh(), across))
        fetch.wait()
        for j in range(np_):
            k = lax.rem(core * 2 + j, 4)
            norm(g, k)
            if j < 2:
                go(pass_tok(g, 0, k, fresh(), beside))
        for c in range(np_):
            cast(1, c)

        have_tok(g, 1, t)
        go(pass_tok(g, 1, t, fresh(), {"tp": x_peer}))
        go(pass_tok(g, 1, t, fresh(), beside))
        go(pass_tok(g, 1, t, fresh(), next_core))
        go(pass_tok(g, 1, t, fresh(), {"tp": cross_peer}))

        def forward(kind, c):
            arrived(kind, outer, c)
            go(weight(kind, outer, c, fresh(), across))

        def hand_on(kind, k):
            have_tok(1 - g, kind, k)
            go(pass_tok(1 - g, kind, k, fresh(), next_core))

        forward(0, 0)
        hand_on(0, core * 2)
        forward(0, 1)
        hand_on(0, core * 2 + 1)
        have_tok(g, 1, x_peer)
        go(pass_tok(g, 1, x_peer, fresh(), beside))
        forward(0, 2)
        forward(0, 3)
        for c in range(np_):
            go(weight(1, z, c, fresh(), across))

        tile = 256
        most = 3 * depth
        low, rest = pair * depth, outer2 * depth
        most_at = pl.ds(pl.multiple_of(low, depth), most)
        rest_at = pl.ds(pl.multiple_of(rest, depth), depth)

        def lift_most(b):
            lines = at(b, rows)

            def one(i, _):
                columns = at(i, tile)
                acc[lines, columns] = jnp.dot(tok[lines, most_at], up[most_at, columns], preferred_element_type=f32)
                return 0
            lax.fori_loop(0, half // tile, one, 0)

        def lift_rest(b):
            lines = at(b, rows)

            def one(i, _):
                columns = at(i, tile)
                lifted = acc[lines, columns] + jnp.dot(tok[lines, rest_at], up[rest_at, columns],
                                                       preferred_element_type=f32)
                whole = pl.ds(pl.multiple_of(g * half + i * tile, tile), tile)
                hid[lines, columns] = activate(lifted, up_scale[:, whole])
                return 0
            lax.fori_loop(0, half // tile, one, 0)

        for c in range(np_):
            arrived(0, other, c)
        lift_most(g)
        have_tok(g, 1, core_peer)
        have_tok(g, 1, cross_peer)
        lift_most(2 + g)
        hand_on(1, t)
        have_tok(1 - g, 0, lax.rem(core * 2 + 2, 4))
        have_tok(1 - g, 0, lax.rem(core * 2 + 3, 4))
        lift_most(1 - g)
        hand_on(1, x_peer)
        have_tok(1 - g, 1, core_peer)
        have_tok(1 - g, 1, cross_peer)
        lift_most(3 - g)
        for c in range(np_):
            arrived(0, outer2, c)
        for b in (g, 2 + g, 1 - g, 3 - g):
            lift_rest(b)
        scales()

        mine, theirs = at(core, 2 * rows), at(1 - core, 2 * rows)
        here, there = at(g, rows), at(1 - g, rows)

        def project(i):
            zz, k, w, _ = units[i]
            b = zz * np_ + k
            weights = down[b] if w == 1 else jnp.concatenate([down[b + j] for j in range(w)], axis=1)
            product = jnp.dot(hid[theirs, :], weights, preferred_element_type=f32).astype(bf)
            for j in range(w):
                core_out[b + j] = product[:, j * dc:(j + 1) * dc]
            go(remote(part(core_out, i), part(core_in, i), fresh(), core_recv.at[i], next_core))
            keep[i % 3, :, pl.ds(0, w * dc)] = jnp.dot(hid[mine, :], weights, preferred_element_type=f32)

        def fold(i):
            zz, k, w, _ = units[i]
            remote(part(core_out, i), part(core_in, i), 0, core_recv.at[i], next_core).wait_recv()
            for j in range(w):
                b, lanes = zz * np_ + k + j, pl.ds(j * dc, dc)
                y_out[b] = (keep[i % 3, there, lanes] + core_in[b, there, :].astype(f32)).astype(bf)
            go(remote(part(y_out, i), part(y_in, i), fresh(), y_recv.at[i], beside))
            for j in range(w):
                b, lanes = zz * np_ + k + j, pl.ds(j * dc, dc)
                keep[i % 3, here, lanes] = keep[i % 3, here, lanes] + core_in[b, here, :].astype(f32)

        away = {"fs": jnp.where(core == 0, z, outer), "tp": jnp.where(core == 0, x_peer, t)}

        def add(i):
            zz, k, w, _ = units[i]
            remote(part(y_out, i), part(y_in, i), 0, y_recv.at[i], beside).wait_recv()
            for j in range(w):
                b, lanes = zz * np_ + k + j, pl.ds(j * dc, dc)
                xz_out[b] = (keep[i % 3, here, lanes] + y_in[b].astype(f32)).astype(bf)
            go(remote(part(xz_out, i), part(x_in, i), fresh(), x_recv.at[i], away))

        def finish(i):
            @pl.when(core == 0)
            def _():
                remote(part(xz_out, i), part(x_in, i), 0, x_recv.at[i], away).wait_recv()
                value(i, xz_out, x_in)
                share(i).start()

        for i in range(n + 3):
            if 0 <= i - 1 < n:
                fold(i - 1)
            if i < n:
                zz, k, w, j = units[i]
                if j:
                    for c in range(k, k + w):
                        if j > 1:
                            arrived(1, zz, c)
                project(i)
            if i < 2:
                forward(1, 2 * i)
                forward(1, 2 * i + 1)
            if 0 <= i - 2 < n:
                add(i - 2)
            if 0 <= i - 3 < n:
                finish(i - 3)
        for copy in started[mark:]:
            copy.wait_send()
        del started[mark:]

        @pl.when(core == 0)
        def _():
            for i in range(n):
                share(i).wait_send()

        @pl.when(core == 1)
        def _():
            for i in range(n):
                share(i).wait_recv()

    for copy in started:
        copy.wait_send()

    step = 64

    def result(i):
        place = pl.ds(pl.multiple_of(i * step, step), step)
        return pltpu.make_async_copy(res.at[place, :], out.at[place, :], out_sem.at[i])

    def close(i, _):
        place = pl.ds(pl.multiple_of(i * step, step), step)
        row = jnp.concatenate([branch[b, place, :] for b in range(4 * np_)], axis=1).astype(f32)
        res[place, :] = (res[place, :].astype(f32) + rms_rows(row, post_gain[...])).astype(bf)
        result(i).start()
        return 0

    lax.fori_loop(0, rows // step, close, 0)
    for i in range(rows // step):
        result(i).wait()


def fused(tokens, pre_gain, up_weight, up_scale, down_weight, down_scale, post_gain):
    rows, width = tokens.shape
    depth, ff = up_weight.shape
    half, dc = ff // 2, depth // PIECES
    pieces = 4 * PIECES
    n = sum(len(w) for w in WIDTHS)
    bf, f32 = jnp.bfloat16, jnp.float32
    dma = pltpu.SemaphoreType.DMA
    anywhere, vmem = pl.BlockSpec(memory_space=pl.ANY), pl.BlockSpec(memory_space=pltpu.VMEM)
    return pl.pallas_call(
        kernel,
        out_shape=jax.ShapeDtypeStruct((rows, width), bf),
        in_specs=[anywhere, anywhere, anywhere, vmem, vmem, vmem, vmem],
        out_specs=anywhere,
        scratch_shapes=[
            pltpu.VMEM((rows, width), bf),
            pltpu.VMEM((depth, half), f32),
            pltpu.VMEM((half, depth), f32),
            pltpu.VMEM((width, half), bf),
            pltpu.VMEM((pieces, half, dc), bf),
            pltpu.VMEM((4 * rows, width), bf),
            pltpu.VMEM((4 * rows, half), f32),
            pltpu.VMEM((4 * rows, half), bf),
            pltpu.VMEM((4, 1, depth), f32),
            pltpu.VMEM((3, 2 * rows, 2 * dc), f32),
            pltpu.VMEM((pieces, 2 * rows, dc), bf),
            pltpu.VMEM((pieces, 2 * rows, dc), bf),
            pltpu.VMEM((pieces, rows, dc), bf),
            pltpu.VMEM((pieces, rows, dc), bf),
            pltpu.VMEM((pieces, rows, dc), bf),
            pltpu.VMEM((pieces, rows, dc), bf),
            pltpu.VMEM((pieces, rows, dc), bf),
            dma((144,)),
            dma((4, PIECES)),
            dma((4, PIECES)),
            dma((4, PIECES)),
            dma((4,)),
            dma((n,)),
            dma((n,)),
            dma((n,)),
            dma((n,)),
            dma((2, PIECES)),
            dma((2,)),
            dma((8,)),
        ],
        compiler_params=pltpu.CompilerParams(
            collective_id=0, has_side_effects=True, vmem_limit_bytes=60 << 20
        ),
    )(tokens, up_weight, down_weight, up_scale.reshape(1, ff), down_scale.reshape(1, depth),
      pre_gain.reshape(1, width), post_gain.reshape(1, width))


def solution(mesh):
    placed = (P(("grp", "fs"), None), P(), P("fs", "tp"), P("tp"), P("tp", "fs"), P("fs"), P())
    sizes = mesh.shape
    line = sizes["grp"] == 2 and sizes["fs"] == 4 and sizes["tp"] == 4
    return jax.shard_map(
        fused if line else plain, mesh=mesh, in_specs=placed, out_specs=P(("grp", "fs"), None), check_vma=False
    )
```

time: 150 us -> 126 us (0.84); the launches traced: 148 us -> 126 us
  Pallas kernels: 145 us -> 123 us
    pallas_call x1, Pallas kernels: 145 us -> 123 us  [fused(): pl.pallas_call(kernel, out_shape=jax.ShapeDtypeStruct((rows, width), bf),...]
where the time goes in v1:
time: 126 us
  Pallas kernels  123 us (98%)
  local copies, waits for them, and re-layouts  3.16 us (3%)
    pallas_call x1, Pallas kernels, fused(): pl.pallas_call(kernel, out_shape=jax.ShapeDtypeStruct((rows, width), bf),...  123 us
    unnamed x1, local copies, waits for them, and re-layouts  3.16 us

profile of v1, /device:TPU:0, one launch (start us, length us, event | category | flops | bytes accessed | tf_op | source)
XLA Modules:
  0.0 125.8 jit_solution(5558641280488164651)
XLA Ops:
  0.0 122.6 %shard_map.73 = bf16[512,2048]{1,0:T(8,128)(2,1)} custom-call(bf16[512,2048]{1,0:T(8,128)(2,1)} %tokens.1, f32[512,2048]{1,0:T(8,128)} %up_in.1, f32[2048,512]{1,0:T(8,128)} %down_in.1, f32[1,2048]{1,0:T(1,128)} %bitcast.4, f32[1,512]{1,0:T(1,128)} %bitcast.7, f32[1,2048]{1,0:T(1,128)} %bitcast.5, f32[1,2048]{1,0:T(1,128)} %bitcast.6), custom_call_target="tpu_custom_call" | custom-call | tf_op jit(solution)/shard_map/pallas_call | solution.py:407
  122.6 3.2 %copy.9 = bf16[512,2048]{1,0:T(8,128)(2,1)} copy(bf16[512,2048]{1,0:T(8,128)(2,1)} %shard_map.73) | data formatting | bytes 4194304

commit v2 on v1

v2 whole, which is shorter than its diff:
```python
import jax
import jax.numpy as jnp
from jax import lax
from jax.experimental import pallas as pl
from jax.experimental.pallas import tpu as pltpu
from jax.sharding import PartitionSpec as P

epsilon = 1e-06
MESH = pl.DeviceIdType.MESH
PIECES = 4
WIDTHS = ((2, 2), (2, 2), (2, 2), (2, 1, 1))
RAW = (0, 1, 0, 1, 0, 1, 2, 2, 2)
ARRIVAL = (1, 0, 3, 2, 5, 4, 6, 7, 8)


def rms_rows(values, scaling):
    return values * lax.rsqrt(jnp.mean(values * values, axis=-1, keepdims=True) + epsilon) * scaling


def activate(lifted, up_scale):
    return jnp.square(jax.nn.relu(lifted * up_scale)).astype(jnp.bfloat16)


def plain(tokens, pre_gain, up_weight, up_scale, down_weight, down_scale, post_gain):
    residual = tokens.astype(jnp.float32)
    normed = rms_rows(residual, pre_gain).astype(jnp.bfloat16)
    up_cast = up_weight.astype(jnp.bfloat16)
    down_cast = down_weight.astype(jnp.bfloat16)
    column_scales = lax.all_gather(down_scale, "fs", axis=0, tiled=True)
    up_full, down_full = (
        lax.all_gather(up_cast, "fs", axis=0, tiled=True),
        lax.all_gather(down_cast, "fs", axis=1, tiled=True),
    )
    lifted = jnp.dot(normed, up_full, preferred_element_type=jnp.float32)
    hidden = activate(lifted, up_scale)
    partials = jnp.dot(hidden, down_full, preferred_element_type=jnp.float32)
    partials = (partials * column_scales).astype(jnp.bfloat16)
    summed = lax.psum(partials, "tp").astype(jnp.float32)
    branch = lax.optimization_barrier(summed.astype(jnp.bfloat16)).astype(jnp.float32)
    return (residual + rms_rows(branch, post_gain)).astype(jnp.bfloat16)


def kernel(tokens, up_in, down_in, up_scale, down_scale, pre_gain, post_gain, out, res, up_f32, down_f32, up, down,
           tok, acc, hid, scl, keep, core_out, core_in, y_out, y_in, xz_out, x_in, branch, send, up_recv, down_recv,
           tok_recv, scl_recv, core_recv, y_recv, x_recv, raw_recv, br_recv,
           local, one_sem):
    g, z, t = lax.axis_index("grp"), lax.axis_index("fs"), lax.axis_index("tp")
    core, x = lax.rem(t, 2), t // 2
    pair = z // 2
    outer, inner, other = 3 * pair, 1 + pair, 2 - pair
    outer2 = 3 - outer
    is_outer = z == outer
    n_tp, np_ = 4, PIECES
    rows, width = tokens.shape
    depth, half = up_in.shape[0], up_in.shape[1] // 2
    du, dc, quarter = depth // np_, depth // np_, rows // np_
    core_peer, x_peer, cross_peer = x * 2 + 1 - core, (1 - x) * 2 + core, (1 - x) * 2 + 1 - core
    bf, f32 = jnp.bfloat16, jnp.float32

    def at(i, size):
        return pl.ds(pl.multiple_of(i * size, size), size)

    def load(kind, c):
        if kind == 0:
            copy = up_in.at[pl.ds(c * du, du), at(g, half)], up_f32.at[pl.ds(c * du, du), :]
        else:
            copy = down_in.at[at(g, half), :], down_f32
        return pltpu.make_async_copy(*copy, local.at[np_ if kind else c])

    load(0, 0).start()
    fetch = pltpu.make_async_copy(tokens, res, one_sem.at[0])
    fetch.start()
    for c in range(1, np_):
        load(0, c).start()
    load(1, 0).start()

    barrier = pltpu.get_barrier_semaphore()
    peers = [{"fs": lax.rem(z + o, 4)} for o in range(1, 4)] + [{"grp": 1 - g}]
    peers += [{"tp": lax.rem(t + o, n_tp)} for o in range(1, n_tp)]
    peers += [{"grp": 1 - g, "fs": z + 1 - 2 * lax.rem(z, 2)}]
    for peer in peers:
        pl.semaphore_signal(barrier, inc=1, device_id=peer, device_id_type=MESH)
    pl.semaphore_wait(barrier, len(peers))

    def remote(src, dst, s, r, peer):
        return pltpu.make_async_remote_copy(src_ref=src, dst_ref=dst, send_sem=send.at[s], recv_sem=r,
                                            device_id=peer, device_id_type=MESH)

    def same(ref, s, r, peer):
        return remote(ref, ref, s, r, peer)

    def slot(kind, zz, c, stage):
        if kind == 0:
            return up.at[at(zz * np_ + c, du), :], up_recv.at[c if stage == 0 else 3 + stage]
        mark = 2 * stage + c // 4 if stage < 2 or c < 4 else 5 + max(0, c - 5)
        return down.at[zz * np_ + c // 2, pl.ds(c % 2 * (half // 2), half // 2), :], down_recv.at[mark]

    def cast(kind, c):
        if kind == 0 or c == 0:
            load(kind, c).wait()
        if kind == 0:
            up[at(z * np_ + c, du), :] = up_f32[pl.ds(c * du, du), :].astype(bf)
        else:
            down[z * np_ + c] = down_f32[:, pl.ds(c * dc, dc)].astype(bf)

    def weight(kind, zz, c, stage, s, peer):
        ref, r = slot(kind, zz, c, stage)
        same(ref, s, r, peer).start()

    def took(ref, r):
        same(ref, 0, r, {"fs": other}).wait_recv()

    def gave(ref, s):
        same(ref, s, scl_recv.at[0], {"fs": other}).wait_send()

    def piece(gg, kind, k):
        b = kind * 2 + gg
        return tok.at[at(b * np_ + k, quarter), :], tok_recv.at[b, k]

    def pass_tok(gg, kind, k, peer):
        ref, r = piece(gg, kind, k)
        same(ref, 1, r, peer).start()

    def have_tok(gg, kind, k):
        took(*piece(gg, kind, k))

    def norm(b, k):
        def one(i, _):
            source = pl.ds(pl.multiple_of(k * quarter + i * 64, 64), 64)
            target = pl.ds(pl.multiple_of((b * np_ + k) * quarter + i * 64, 64), 64)
            tok[target, :] = rms_rows(res[source, :].astype(f32), pre_gain[...]).astype(bf)
            return 0
        lax.fori_loop(0, quarter // 64, one, 0)

    blocks = (inner, outer, other, outer2)
    units = []
    for j, widths in enumerate(WIDTHS):
        k = 0
        for w in widths:
            units.append((blocks[j], k, w, j))
            k += w
    n = len(units)

    def total(*modes):
        return sum(u[2] for u, raw in zip(units, RAW) if raw in modes)

    def part(ref, i):
        zz, k, w, _ = units[i]
        return ref.at[pl.ds(zz * np_ + k, w)]

    mine_rows, their_rows = at(g, rows), at(1 - g, rows)

    def half_of(ref, i, lines):
        zz, k, w, _ = units[i]
        return ref.at[pl.ds(zz * np_ + k, w), lines, :]

    def raw_half(i, own, s):
        lines = mine_rows if own else their_rows
        ref = half_of(core_in, i, lines)
        return same(ref, s, (raw_recv if own else core_recv).at[i], {"fs": outer})

    def value(i, first, second):
        zz, k, w, _ = units[i]
        for j in range(w):
            b = zz * np_ + k + j
            total = first[b].astype(f32) + second[b].astype(f32)
            branch[b] = (total * scl[zz, :, pl.ds((k + j) * dc, dc)]).astype(bf)

    def share(i):
        return same(part(branch, i), 2, br_recv.at[0], {"tp": core_peer})

    for o in range(1, 4):
        remote(down_scale, scl.at[z], 0, scl_recv.at[0], {"fs": lax.rem(z + o, 4)}).start()
    own_scale = pltpu.make_async_copy(down_scale, scl.at[z], one_sem.at[1])
    own_scale.start()

    def scales():
        own_scale.wait()
        took(scl.at[pl.ds(0, 3)], scl_recv.at[0])

    @pl.when(is_outer)
    def _():
        to = {"fs": inner}
        fetch.wait()
        norm(2 + g, t)
        pass_tok(g, 1, t, to)
        for c in range(np_):
            cast(0, c)
            weight(0, z, c, 0, 3, to)
        for c in range(np_):
            cast(1, c)
            for k in range(2):
                weight(1, z, 2 * c + k, 0, 4, to)
        scales()

        @pl.when(core == 1)
        def _():
            def relay(i):
                return remote(part(x_in, i), part(y_in, i), 5, y_recv.at[i], {"tp": x_peer})

            def side(i):
                return remote(half_of(core_in, i, their_rows), part(y_in, i), 6, y_recv.at[i], {"grp": 1 - g})

            def swap(i):
                return remote(part(xz_out, i), part(x_in, i), 7, x_recv.at[i], {"tp": x_peer})

            def first(i):
                if RAW[i] == 2:
                    raw_half(i, True, 0).wait_recv()
                elif RAW[i]:
                    raw_half(i, False, 0).wait_recv()
                    side(i).start()
                else:
                    remote(part(x_in, i), part(x_in, i), 0, x_recv.at[i], {"fs": inner}).wait_recv()
                    relay(i).start()

            def second(i):
                zz, k, w, _ = units[i]
                if RAW[i] == 1:
                    raw_half(i, True, 0).wait_recv()
                side(i).wait_recv()
                for j in range(w):
                    b = zz * np_ + k + j
                    xz_out[b] = (core_in[b, mine_rows, :].astype(f32) + y_in[b].astype(f32)).astype(bf)
                swap(i).start()

            def third(i):
                if RAW[i]:
                    swap(i).wait_recv()
                    value(i, xz_out, x_in)
                else:
                    relay(i).wait_recv()
                    value(i, x_in, y_in)
                share(i).start()

            for s in range(n + 2):
                if s < n:
                    first(ARRIVAL[s])
                if 0 <= s - 1 < n:
                    i = ARRIVAL[s - 1]
                    if RAW[i]:
                        second(i)
                    else:
                        third(i)
                if 0 <= s - 2 < n and RAW[ARRIVAL[s - 2]]:
                    third(ARRIVAL[s - 2])
            gave(x_in.at[pl.ds(0, total(0))], 5)
            gave(x_in.at[pl.ds(0, total(1))], 6)
            gave(x_in.at[pl.ds(0, total(1, 2))], 7)
            gave(branch, 2)

        @pl.when(core == 0)
        def _():
            took(branch, br_recv.at[0])

        gave(tok.at[pl.ds(0, quarter), :], 1)
        gave(up.at[pl.ds(0, depth), :], 3)
        gave(down.at[pl.ds(0, np_)], 4)

    @pl.when(jnp.logical_not(is_outer))
    def _():
        across, beside, next_core = {"fs": other}, {"grp": 1 - g}, {"tp": core_peer}
        for c in range(np_):
            cast(0, c)
            weight(0, z, c, 1, 3, across)
        fetch.wait()
        for j in range(np_):
            k = lax.rem(core * 2 + j, 4)
            norm(g, k)
            if j < 2:
                pass_tok(g, 0, k, beside)
        for c in range(np_):
            cast(1, c)

        have_tok(g, 1, t)
        for peer in ({"tp": x_peer}, beside, next_core, {"tp": cross_peer}):
            pass_tok(g, 1, t, peer)

        def forward(c):
            took(*slot(0, outer, c, 0))
            weight(0, outer, c, 2, 4, across)

        def forward_down(c):
            took(down.at[pl.ds(outer * np_ + 2 * c, 2)], down_recv.at[c])
            for k in range(4):
                weight(1, outer, 4 * c + k, 2, 6, across)

        def hand_on(kind, k):
            have_tok(1 - g, kind, k)
            pass_tok(1 - g, kind, k, next_core)

        forward(0)
        hand_on(0, core * 2)
        forward(1)
        hand_on(0, core * 2 + 1)
        have_tok(g, 1, x_peer)
        pass_tok(g, 1, x_peer, beside)
        forward(2)
        forward(3)
        for c in range(2 * np_):
            weight(1, z, c, 1, 5, across)

        tile = 512
        most = 3 * depth
        low, rest = pair * depth, outer2 * depth
        most_at = pl.ds(pl.multiple_of(low, depth), most)
        rest_at = pl.ds(pl.multiple_of(rest, depth), depth)

        def lift_most(b):
            lines = at(b, rows)

            def one(i, _):
                columns = at(i, tile)
                acc[lines, columns] = jnp.dot(tok[lines, most_at], up[most_at, columns], preferred_element_type=f32)
                return 0
            lax.fori_loop(0, half // tile, one, 0)

        def lift_all(b):
            lines = at(b, rows)

            def one(i, _):
                columns = at(i, tile)
                lifted = jnp.dot(tok[lines, :], up[:, columns], preferred_element_type=f32)
                whole = pl.ds(pl.multiple_of(g * half + i * tile, tile), tile)
                hid[lines, columns] = activate(lifted, up_scale[:, whole])
                return 0
            lax.fori_loop(0, half // tile, one, 0)

        def lift_rest(b):
            lines = at(b, rows)

            def one(i, _):
                columns = at(i, tile)
                lifted = acc[lines, columns] + jnp.dot(tok[lines, rest_at], up[rest_at, columns],
                                                       preferred_element_type=f32)
                whole = pl.ds(pl.multiple_of(g * half + i * tile, tile), tile)
                hid[lines, columns] = activate(lifted, up_scale[:, whole])
                return 0
            lax.fori_loop(0, half // tile, one, 0)

        took(up.at[at(other, depth), :], up_recv.at[4])
        lift_most(g)
        have_tok(g, 1, core_peer)
        have_tok(g, 1, cross_peer)
        lift_most(2 + g)
        hand_on(1, t)
        have_tok(1 - g, 0, lax.rem(core * 2 + 2, 4))
        have_tok(1 - g, 0, lax.rem(core * 2 + 3, 4))
        lift_most(1 - g)
        hand_on(1, x_peer)
        took(up.at[at(outer2, depth), :], up_recv.at[5])
        for b in (g, 2 + g, 1 - g):
            lift_rest(b)
        have_tok(1 - g, 1, core_peer)
        have_tok(1 - g, 1, cross_peer)
        lift_all(3 - g)
        scales()

        mine, theirs = at(core, 2 * rows), at(1 - core, 2 * rows)
        def project(i):
            zz, k, w, _ = units[i]
            b = zz * np_ + k
            weights = down[b] if w == 1 else jnp.concatenate([down[b + j] for j in range(w)], axis=1)
            product = jnp.dot(hid[theirs, :], weights, preferred_element_type=f32).astype(bf)
            for j in range(w):
                core_out[b + j] = product[:, j * dc:(j + 1) * dc]
            remote(part(core_out, i), part(core_in, i), 7, core_recv.at[i], next_core).start()
            keep[i % 3, :, pl.ds(0, w * dc)] = jnp.dot(hid[mine, :], weights, preferred_element_type=f32)

        def project_last(i):
            zz, k, _, _ = units[i]
            b = zz * np_ + k
            early, late = pl.ds(0, half // 2), pl.ds(half // 2, half // 2)
            lanes = pl.ds(0, dc)
            took(*slot(1, zz, 2 * k, 2))
            acc[pl.ds(0, 2 * rows), lanes] = jnp.dot(hid[theirs, early], down[b, early, :], preferred_element_type=f32)
            keep[i % 3, :, lanes] = jnp.dot(hid[mine, early], down[b, early, :], preferred_element_type=f32)
            took(*slot(1, zz, 2 * k + 1, 2))
            core_out[b] = (acc[pl.ds(0, 2 * rows), lanes] + jnp.dot(
                hid[theirs, late], down[b, late, :], preferred_element_type=f32)).astype(bf)
            remote(part(core_out, i), part(core_in, i), 7, core_recv.at[i], next_core).start()
            keep[i % 3, :, lanes] = keep[i % 3, :, lanes] + jnp.dot(
                hid[mine, late], down[b, late, :], preferred_element_type=f32)

        away = {"fs": jnp.where(core == 0, z, outer), "tp": jnp.where(core == 0, x_peer, t)}

        def by_y(i):
            return remote(part(y_out, i), part(y_in, i), 8, y_recv.at[i], beside)

        def direct(i):
            return remote(half_of(core_in, i, their_rows), part(y_in, i), 10, y_recv.at[i],
                          {"grp": 1 - g, "fs": outer})

        def sent_away(i):
            return remote(part(xz_out, i), part(x_in, i), 9, x_recv.at[i], away)

        def fold(i):
            zz, k, w, _ = units[i]
            remote(part(core_out, i), part(core_in, i), 0, core_recv.at[i], next_core).wait_recv()

            def pieces(lines):
                for j in range(w):
                    b = zz * np_ + k + j
                    yield b, keep[i % 3, lines, pl.ds(j * dc, dc)] + core_in[b, lines, :].astype(f32)

            def through_y():
                for b, total in pieces(their_rows):
                    y_out[b] = total.astype(bf)
                by_y(i).start()
                for j in range(w):
                    b, lanes = zz * np_ + k + j, pl.ds(j * dc, dc)
                    keep[i % 3, mine_rows, lanes] = (keep[i % 3, mine_rows, lanes]
                                                     + core_in[b, mine_rows, :].astype(f32))

            if not RAW[i]:
                through_y()
                return

            @pl.when(core == 0)
            def _():
                through_y()

            @pl.when(core == 1)
            def _():
                for own in range(2):
                    lines = mine_rows if own else their_rows
                    for b, total in pieces(lines):
                        core_in[b, lines, :] = total.astype(bf)
                    if RAW[i] == 2 and not own:
                        direct(i).start()
                    else:
                        raw_half(i, own, 10).start()

        def add(i):
            zz, k, w, _ = units[i]

            def through_x():
                by_y(i).wait_recv()
                for j in range(w):
                    b, lanes = zz * np_ + k + j, pl.ds(j * dc, dc)
                    xz_out[b] = (keep[i % 3, mine_rows, lanes] + y_in[b].astype(f32)).astype(bf)
                sent_away(i).start()

            if not RAW[i]:
                through_x()
                return

            @pl.when(core == 0)
            def _():
                through_x()

        def finish(i):
            @pl.when(core == 0)
            def _():
                sent_away(i).wait_recv()
                value(i, xz_out, x_in)
                share(i).start()

        def ready(i):
            zz, k, w, j = units[i]
            if j > 1:
                took(down.at[pl.ds(zz * np_ + k, w)], slot(1, zz, 2 * k, j - 1)[1])

        for i in range(n):
            eager = units[i][3] == 3
            if i and not eager:
                fold(i - 1)
            if eager and units[i - 1][3] < 3:
                fold(i - 1)
                add(i - 2)
                finish(i - 3)
            if i == n - 1:
                project_last(i)
            else:
                ready(i)
                project(i)
            if i < 2:
                forward_down(i)
            if eager:
                fold(i)
                add(i - 1)
                finish(i - 2)
            else:
                if i >= 2:
                    add(i - 2)
                if i >= 3:
                    finish(i - 3)
        add(n - 1)
        finish(n - 2)
        finish(n - 1)
        gave(tok.at[pl.ds(0, 11 * quarter), :], 1)
        for s in (3, 4):
            gave(up.at[pl.ds(0, depth), :], s)
        for s in (5, 6):
            gave(down.at[pl.ds(0, np_)], s)
        gave(core_out, 7)

        @pl.when(core == 0)
        def _():
            gave(y_out, 8)
            gave(xz_out, 9)
            gave(branch, 2)

        @pl.when(core == 1)
        def _():
            gave(y_out.at[pl.ds(0, total(0))], 8)
            gave(xz_out.at[pl.ds(0, total(0))], 9)
            gave(core_in.at[pl.ds(0, total(1, 2))], 10)
            took(branch, br_recv.at[0])

    gave(scl.at[pl.ds(0, 3)], 0)

    step = 64

    def result(i):
        place = pl.ds(pl.multiple_of(i * step, step), step)
        return pltpu.make_async_copy(res.at[place, :], out.at[place, :], one_sem.at[2])

    def close(i, _):
        place = pl.ds(pl.multiple_of(i * step, step), step)
        row = jnp.concatenate([branch[b, place, :] for b in range(4 * np_)], axis=1).astype(f32)
        res[place, :] = (res[place, :].astype(f32) + rms_rows(row, post_gain[...])).astype(bf)
        result(i).start()
        return 0

    lax.fori_loop(0, rows // step, close, 0)
    pltpu.make_async_copy(res, out, one_sem.at[2]).wait()


def fused(tokens, pre_gain, up_weight, up_scale, down_weight, down_scale, post_gain):
    rows, width = tokens.shape
    depth, ff = up_weight.shape
    half, dc = ff // 2, depth // PIECES
    pieces = 4 * PIECES
    n = sum(len(w) for w in WIDTHS)
    bf, f32 = jnp.bfloat16, jnp.float32
    dma = pltpu.SemaphoreType.DMA
    anywhere, vmem = pl.BlockSpec(memory_space=pl.ANY), pl.BlockSpec(memory_space=pltpu.VMEM)
    return pl.pallas_call(
        kernel,
        out_shape=jax.ShapeDtypeStruct((rows, width), bf),
        in_specs=[anywhere, anywhere, anywhere, vmem, vmem, vmem, vmem],
        out_specs=anywhere,
        scratch_shapes=[
            pltpu.VMEM((rows, width), bf),
            pltpu.VMEM((depth, half), f32),
            pltpu.VMEM((half, depth), f32),
            pltpu.VMEM((width, half), bf),
            pltpu.VMEM((pieces, half, dc), bf),
            pltpu.VMEM((4 * rows, width), bf),
            pltpu.VMEM((4 * rows, half), f32),
            pltpu.VMEM((4 * rows, half), bf),
            pltpu.VMEM((4, 1, depth), f32),
            pltpu.VMEM((3, 2 * rows, 2 * dc), f32),
            pltpu.VMEM((pieces, 2 * rows, dc), bf),
            pltpu.VMEM((pieces, 2 * rows, dc), bf),
            pltpu.VMEM((pieces, rows, dc), bf),
            pltpu.VMEM((pieces, rows, dc), bf),
            pltpu.VMEM((pieces, rows, dc), bf),
            pltpu.VMEM((pieces, rows, dc), bf),
            pltpu.VMEM((pieces, rows, dc), bf),
            dma((11,)),
            dma((6,)),
            dma((8,)),
            dma((4, PIECES)),
            dma((1,)),
            dma((n,)),
            dma((n,)),
            dma((n,)),
            dma((n,)),
            dma((1,)),
            dma((PIECES + 1,)),
            dma((3,)),
        ],
        compiler_params=pltpu.CompilerParams(
            collective_id=0, has_side_effects=True, vmem_limit_bytes=60 << 20
        ),
    )(tokens, up_weight, down_weight, up_scale.reshape(1, ff), down_scale.reshape(1, depth),
      pre_gain.reshape(1, width), post_gain.reshape(1, width))


def solution(mesh):
    placed = (P(("grp", "fs"), None), P(), P("fs", "tp"), P("tp"), P("tp", "fs"), P("fs"), P())
    sizes = mesh.shape
    line = sizes["grp"] == 2 and sizes["fs"] == 4 and sizes["tp"] == 4
    return jax.shard_map(
        fused if line else plain, mesh=mesh, in_specs=placed, out_specs=P(("grp", "fs"), None), check_vma=False
    )
```

time: 126 us -> 116 us (0.921)
  Pallas kernels: 123 us -> 113 us
    pallas_call x1, Pallas kernels: 123 us -> 113 us  [fused(): pl.pallas_call(kernel, out_shape=jax.ShapeDtypeStruct((rows, width), bf),...]
where the time goes in v2:
time: 116 us
  Pallas kernels  113 us (97%)
  local copies, waits for them, and re-layouts  3.16 us (3%)
    pallas_call x1, Pallas kernels, fused(): pl.pallas_call(kernel, out_shape=jax.ShapeDtypeStruct((rows, width), bf),...  113 us
    unnamed x1, local copies, waits for them, and re-layouts  3.16 us

profile of v2, /device:TPU:0, one launch (start us, length us, event | category | flops | bytes accessed | tf_op | source)
XLA Modules:
  0.0 115.9 jit_solution(3932358472189284637)
XLA Ops:
  0.0 112.7 %shard_map.73 = bf16[512,2048]{1,0:T(8,128)(2,1)} custom-call(bf16[512,2048]{1,0:T(8,128)(2,1)} %tokens.1, f32[512,2048]{1,0:T(8,128)} %up_in.1, f32[2048,512]{1,0:T(8,128)} %down_in.1, f32[1,2048]{1,0:T(1,128)} %bitcast.4, f32[1,512]{1,0:T(1,128)} %bitcast.7, f32[1,2048]{1,0:T(1,128)} %bitcast.5, f32[1,2048]{1,0:T(1,128)} %bitcast.6), custom_call_target="tpu_custom_call" | custom-call | tf_op jit(solution)/shard_map/pallas_call | solution.py:539
  112.7 3.2 %copy.9 = bf16[512,2048]{1,0:T(8,128)(2,1)} copy(bf16[512,2048]{1,0:T(8,128)(2,1)} %shard_map.73) | data formatting | bytes 4194304

commit v3 on v2

--- a/solution.py
+++ b/solution.py
@@ -10,7 +10,9 @@
 PIECES = 4
 WIDTHS = ((2, 2), (2, 2), (2, 2), (2, 1, 1))
 RAW = (0, 1, 0, 1, 0, 1, 2, 2, 2)
-ARRIVAL = (1, 0, 3, 2, 5, 4, 6, 7, 8)
+ORDER = ("P0F0P1F1P2F2A0P3F3A1N0P4F4A2P5F5A3N1", "A4N2P6F6A5N3P7F7A6N4P8F8A7N5A8N6N7N8")
+STEPS = tuple(part[i:i + 2] for part in ORDER for i in range(0, len(part), 2))
+ARRIVAL = tuple(int(s[1:]) for s in STEPS if s[0] == "AFFA"[RAW[int(s[1:])]])
 
 
 def rms_rows(values, scaling):
@@ -40,7 +42,7 @@
     return (residual + rms_rows(branch, post_gain)).astype(jnp.bfloat16)
 
 
-def kernel(tokens, up_in, down_in, up_scale, down_scale, pre_gain, post_gain, out, res, up_f32, down_f32, up, down,
+def kernel(tokens, up_in, down_in, up_scale, down_scale, pre_gain, out, res, up_f32, down_f32, up, down,
            tok, acc, hid, scl, keep, core_out, core_in, y_out, y_in, xz_out, x_in, branch, send, up_recv, down_recv,
            tok_recv, scl_recv, core_recv, y_recv, x_recv, raw_recv, br_recv,
            local, one_sem):
@@ -154,6 +156,11 @@
         zz, k, w, _ = units[i]
         return ref.at[pl.ds(zz * np_ + k, w), lines, :]
 
+    fold_rows = rows // 2
+
+    def strip(ref, i, gg):
+        return half_of(ref, i, at(gg, fold_rows))
+
     def raw_half(i, own, s):
         lines = mine_rows if own else their_rows
         ref = half_of(core_in, i, lines)
@@ -166,8 +173,16 @@
             total = first[b].astype(f32) + second[b].astype(f32)
             branch[b] = (total * scl[zz, :, pl.ds((k + j) * dc, dc)]).astype(bf)
 
+    def write(i):
+        pltpu.make_async_copy(part(branch, i), part(out, i), one_sem.at[2]).start()
+
+    def receive(order):
+        for i in order:
+            took(part(branch, i), br_recv.at[i])
+            write(i)
+
     def share(i):
-        return same(part(branch, i), 2, br_recv.at[0], {"tp": core_peer})
+        return same(part(branch, i), 2, br_recv.at[i], {"tp": core_peer})
 
     for o in range(1, 4):
         remote(down_scale, scl.at[z], 0, scl_recv.at[0], {"fs": lax.rem(z + o, 4)}).start()
@@ -204,8 +219,17 @@
             def swap(i):
                 return remote(part(xz_out, i), part(x_in, i), 7, x_recv.at[i], {"tp": x_peer})
 
+            def side_strip(i):
+                return remote(strip(x_in, i, 1 - g), strip(y_in, i, 0), 9, y_recv.at[i], {"grp": 1 - g})
+
+            def swap_strip(i, xx):
+                return same(strip(branch, i, xx), 8, x_recv.at[i], {"tp": x_peer})
+
             def first(i):
-                if RAW[i] == 2:
+                if RAW[i] == 3:
+                    took(strip(x_in, i, 1 - g), core_recv.at[i])
+                    side_strip(i).start()
+                elif RAW[i] == 2:
                     raw_half(i, True, 0).wait_recv()
                 elif RAW[i]:
                     raw_half(i, False, 0).wait_recv()
@@ -216,6 +240,15 @@
 
             def second(i):
                 zz, k, w, _ = units[i]
+                if RAW[i] == 3:
+                    took(strip(x_in, i, g), raw_recv.at[i])
+                    side_strip(i).wait_recv()
+                    for j in range(w):
+                        b = zz * np_ + k + j
+                        both = x_in[b, at(g, fold_rows), :].astype(f32) + y_in[b, pl.ds(0, fold_rows), :].astype(f32)
+                        branch[b, at(x, fold_rows), :] = (both * scl[zz, :, pl.ds((k + j) * dc, dc)]).astype(bf)
+                    swap_strip(i, x).start()
+                    return
                 if RAW[i] == 1:
                     raw_half(i, True, 0).wait_recv()
                 side(i).wait_recv()
@@ -225,13 +258,16 @@
                 swap(i).start()
 
             def third(i):
-                if RAW[i]:
+                if RAW[i] == 3:
+                    swap_strip(i, 1 - x).wait_recv()
+                elif RAW[i]:
                     swap(i).wait_recv()
                     value(i, xz_out, x_in)
                 else:
                     relay(i).wait_recv()
                     value(i, x_in, y_in)
                 share(i).start()
+                write(i)
 
             for s in range(n + 2):
                 if s < n:
@@ -245,13 +281,17 @@
                 if 0 <= s - 2 < n and RAW[ARRIVAL[s - 2]]:
                     third(ARRIVAL[s - 2])
             gave(x_in.at[pl.ds(0, total(0))], 5)
-            gave(x_in.at[pl.ds(0, total(1))], 6)
+            if total(1):
+                gave(x_in.at[pl.ds(0, total(1))], 6)
+            if total(3):
+                for s in (8, 9):
+                    gave(x_in.at[pl.ds(0, total(3)), pl.ds(0, fold_rows), :], s)
             gave(x_in.at[pl.ds(0, total(1, 2))], 7)
             gave(branch, 2)
 
         @pl.when(core == 0)
         def _():
-            took(branch, br_recv.at[0])
+            receive(ARRIVAL)
 
         gave(tok.at[pl.ds(0, quarter), :], 1)
         gave(up.at[pl.ds(0, depth), :], 3)
@@ -364,8 +404,8 @@
             product = jnp.dot(hid[theirs, :], weights, preferred_element_type=f32).astype(bf)
             for j in range(w):
                 core_out[b + j] = product[:, j * dc:(j + 1) * dc]
+            keep[i % 3, :, pl.ds(0, w * dc)] = jnp.dot(hid[mine, :], weights, preferred_element_type=f32)
             remote(part(core_out, i), part(core_in, i), 7, core_recv.at[i], next_core).start()
-            keep[i % 3, :, pl.ds(0, w * dc)] = jnp.dot(hid[mine, :], weights, preferred_element_type=f32)
 
         def project_last(i):
             zz, k, _, _ = units[i]
@@ -387,6 +427,10 @@
         def by_y(i):
             return remote(part(y_out, i), part(y_in, i), 8, y_recv.at[i], beside)
 
+        def turn(i, gg):
+            lines = pl.ds(pl.multiple_of(gg * rows + (1 - x) * fold_rows, fold_rows), fold_rows)
+            return remote(half_of(core_in, i, lines), strip(y_in, i, gg), 11, y_recv.at[i], {"tp": x_peer})
+
         def direct(i):
             return remote(half_of(core_in, i, their_rows), part(y_in, i), 10, y_recv.at[i],
                           {"grp": 1 - g, "fs": outer})
@@ -404,8 +448,8 @@
                     yield b, keep[i % 3, lines, pl.ds(j * dc, dc)] + core_in[b, lines, :].astype(f32)
 
             def through_y():
-                for b, total in pieces(their_rows):
-                    y_out[b] = total.astype(bf)
+                for b, amount in pieces(their_rows):
+                    y_out[b] = amount.astype(bf)
                 by_y(i).start()
                 for j in range(w):
                     b, lanes = zz * np_ + k + j, pl.ds(j * dc, dc)
@@ -416,16 +460,23 @@
                 through_y()
                 return
 
+            def put(lines):
+                for b, amount in pieces(lines):
+                    core_in[b, lines, :] = amount.astype(bf)
+
             @pl.when(core == 0)
             def _():
                 through_y()
 
             @pl.when(core == 1)
             def _():
+                if RAW[i] == 3:
+                    for gg in range(2):
+                        put(pl.ds(gg * rows, rows))
+                        turn(i, gg).start()
+                    return
                 for own in range(2):
-                    lines = mine_rows if own else their_rows
-                    for b, total in pieces(lines):
-                        core_in[b, lines, :] = total.astype(bf)
+                    put(mine_rows if own else their_rows)
                     if RAW[i] == 2 and not own:
                         direct(i).start()
                     else:
@@ -449,45 +500,46 @@
             def _():
                 through_x()
 
+            if RAW[i] == 3:
+                @pl.when(core == 1)
+                def _():
+                    took(part(y_in, i), y_recv.at[i])
+                    for own in range(2):
+                        gg = g if own else 1 - g
+                        lines = at(gg, fold_rows)
+                        kept = pl.ds(pl.multiple_of(gg * rows + x * fold_rows, fold_rows), fold_rows)
+                        for j in range(w):
+                            b = zz * np_ + k + j
+                            xz_out[b, lines, :] = (core_in[b, kept, :].astype(f32)
+                                                   + y_in[b, lines, :].astype(f32)).astype(bf)
+                        remote(strip(xz_out, i, gg), strip(x_in, i, gg), 12, (raw_recv if own else core_recv).at[i],
+                               {"fs": outer}).start()
+
         def finish(i):
             @pl.when(core == 0)
             def _():
                 sent_away(i).wait_recv()
                 value(i, xz_out, x_in)
                 share(i).start()
+                write(i)
 
         def ready(i):
             zz, k, w, j = units[i]
             if j > 1:
                 took(down.at[pl.ds(zz * np_ + k, w)], slot(1, zz, 2 * k, j - 1)[1])
 
-        for i in range(n):
-            eager = units[i][3] == 3
-            if i and not eager:
-                fold(i - 1)
-            if eager and units[i - 1][3] < 3:
-                fold(i - 1)
-                add(i - 2)
-                finish(i - 3)
-            if i == n - 1:
-                project_last(i)
+        for s in STEPS:
+            i = int(s[1:])
+            if s[0] == "P":
+                if i == n - 1:
+                    project_last(i)
+                else:
+                    ready(i)
+                    project(i)
+                if i < 2:
+                    forward_down(i)
             else:
-                ready(i)
-                project(i)
-            if i < 2:
-                forward_down(i)
-            if eager:
-                fold(i)
-                add(i - 1)
-                finish(i - 2)
-            else:
-                if i >= 2:
-                    add(i - 2)
-                if i >= 3:
-                    finish(i - 3)
-        add(n - 1)
-        finish(n - 2)
-        finish(n - 1)
+                {"F": fold, "A": add, "N": finish}[s[0]](i)
         gave(tok.at[pl.ds(0, 11 * quarter), :], 1)
         for s in (3, 4):
             gave(up.at[pl.ds(0, depth), :], s)
@@ -506,25 +558,42 @@
             gave(y_out.at[pl.ds(0, total(0))], 8)
             gave(xz_out.at[pl.ds(0, total(0))], 9)
             gave(core_in.at[pl.ds(0, total(1, 2))], 10)
-            took(branch, br_recv.at[0])
+            if total(3):
+                gave(y_in.at[pl.ds(0, total(3))], 11)
+                gave(xz_out.at[pl.ds(0, total(3))], 12)
+            receive(range(n))
 
     gave(scl.at[pl.ds(0, 3)], 0)
-
-    step = 64
-
-    def result(i):
-        place = pl.ds(pl.multiple_of(i * step, step), step)
-        return pltpu.make_async_copy(res.at[place, :], out.at[place, :], one_sem.at[2])
-
-    def close(i, _):
-        place = pl.ds(pl.multiple_of(i * step, step), step)
-        row = jnp.concatenate([branch[b, place, :] for b in range(4 * np_)], axis=1).astype(f32)
-        res[place, :] = (res[place, :].astype(f32) + rms_rows(row, post_gain[...])).astype(bf)
-        result(i).start()
+    pltpu.make_async_copy(branch, out, one_sem.at[2]).wait()
+
+
+def closing(branch, tokens, post_gain, out, rows_in, rows_out, arrive, bring, leave):
+    parts = arrive.shape[0]
+    step = tokens.shape[0] // parts
+
+    def place(i):
+        return pl.ds(pl.multiple_of(i * step, step), step)
+
+    def fetch(i):
+        return pltpu.make_async_copy(branch.at[:, place(i), :], rows_in.at[:, place(i), :], arrive.at[i])
+
+    def residual(i):
+        return pltpu.make_async_copy(tokens.at[place(i), :], rows_out.at[place(i), :], bring.at[i])
+
+    for i in range(parts):
+        fetch(i).start()
+        residual(i).start()
+
+    def one(i, _):
+        fetch(i).wait()
+        residual(i).wait()
+        row = jnp.concatenate([rows_in[b, place(i), :] for b in range(branch.shape[0])], axis=1).astype(jnp.float32)
+        rows_out[place(i), :] = (rows_out[place(i), :].astype(jnp.float32) + rms_rows(row, post_gain[...])).astype(jnp.bfloat16)
+        pltpu.make_async_copy(rows_out.at[place(i), :], out.at[place(i), :], leave.at[0]).start()
         return 0
 
-    lax.fori_loop(0, rows // step, close, 0)
-    pltpu.make_async_copy(res, out, one_sem.at[2]).wait()
+    lax.fori_loop(0, parts, one, 0)
+    pltpu.make_async_copy(rows_out, out, leave.at[0]).wait()
 
 
 def fused(tokens, pre_gain, up_weight, up_scale, down_weight, down_scale, post_gain):
@@ -536,10 +605,10 @@
     bf, f32 = jnp.bfloat16, jnp.float32
     dma = pltpu.SemaphoreType.DMA
     anywhere, vmem = pl.BlockSpec(memory_space=pl.ANY), pl.BlockSpec(memory_space=pltpu.VMEM)
-    return pl.pallas_call(
+    branch = pl.pallas_call(
         kernel,
-        out_shape=jax.ShapeDtypeStruct((rows, width), bf),
-        in_specs=[anywhere, anywhere, anywhere, vmem, vmem, vmem, vmem],
+        out_shape=jax.ShapeDtypeStruct((pieces, rows, dc), bf),
+        in_specs=[anywhere, anywhere, anywhere, vmem, vmem, vmem],
         out_specs=anywhere,
         scratch_shapes=[
             pltpu.VMEM((rows, width), bf),
@@ -559,7 +628,7 @@
             pltpu.VMEM((pieces, rows, dc), bf),
             pltpu.VMEM((pieces, rows, dc), bf),
             pltpu.VMEM((pieces, rows, dc), bf),
-            dma((11,)),
+            dma((13,)),
             dma((6,)),
             dma((8,)),
             dma((4, PIECES)),
@@ -568,15 +637,25 @@
             dma((n,)),
             dma((n,)),
             dma((n,)),
-            dma((1,)),
+            dma((n,)),
             dma((PIECES + 1,)),
             dma((3,)),
         ],
         compiler_params=pltpu.CompilerParams(
-            collective_id=0, has_side_effects=True, vmem_limit_bytes=60 << 20
+            collective_id=0, has_side_effects=True, vmem_limit_bytes=58 << 20
         ),
     )(tokens, up_weight, down_weight, up_scale.reshape(1, ff), down_scale.reshape(1, depth),
-      pre_gain.reshape(1, width), post_gain.reshape(1, width))
+      pre_gain.reshape(1, width))
+    parts = 8
+    far = pl.BlockSpec(memory_space=pltpu.HBM)
+    return pl.pallas_call(
+        closing,
+        out_shape=jax.ShapeDtypeStruct((rows, width), bf),
+        in_specs=[far, far, vmem],
+        out_specs=far,
+        scratch_shapes=[pltpu.VMEM((pieces, rows, dc), bf), pltpu.VMEM((rows, width), bf), dma((parts,)), dma((parts,)), dma((1,))],
+        compiler_params=pltpu.CompilerParams(vmem_limit_bytes=60 << 20),
+    )(branch, tokens, post_gain.reshape(1, width))
 
 
 def solution(mesh):

time: 116 us -> 116 us (level)
  local copies, waits for them, and re-layouts: 3.16 us -> 0 us
  Pallas kernels: 113 us -> 115 us
    unnamed x1 -> x0, local copies, waits for them, and re-layouts: 3.16 us -> none
    pallas_call x1 -> x2, Pallas kernels: 113 us -> 115 us  [the longest x1 111 us: fused(): pl.pallas_call(kernel, out_shape=jax.ShapeDtypeStruct((pieces, rows, dc),...]
where the time goes in v3:
time: 116 us
  Pallas kernels  115 us (99%)
    pallas_call x1, Pallas kernels, fused(): pl.pallas_call(kernel, out_shape=jax.ShapeDtypeStruct((pieces, rows, dc),...  111 us
    pallas_call x1, Pallas kernels, fused(): pl.pallas_call(closing, out_shape=jax.ShapeDtypeStruct((rows, width), bf)...  4.11 us

profile of v3, /device:TPU:0, one launch (start us, length us, event | category | flops | bytes accessed | tf_op | source)
XLA Modules:
  0.0 115.5 jit_solution(2771839083446783733)
XLA Ops:
  0.0 111.2 %shard_map.73.branch = bf16[16,512,128]{2,1,0:T(8,128)(2,1)} custom-call(bf16[512,2048]{1,0:T(8,128)(2,1)} %tokens.3, f32[512,2048]{1,0:T(8,128)} %up_in.1, f32[2048,512]{1,0:T(8,128)} %down_in.1, f32[1,2048]{1,0:T(1,128)} %bitcast.5, f32[1,512]{1,0:T(1,128)} %bitcast.7, f32[1,2048]{1,0:T(1,128)} %bitcast.6), custom_call_target="tpu_custom_call" | custom-call | tf_op jit(solution)/shard_map/pallas_call | solution.py:608
  111.2 4.1 %shard_map.74 = bf16[512,2048]{1,0:T(8,128)(2,1)} custom-call(bf16[16,512,128]{2,1,0:T(8,128)(2,1)} %shard_map.73.branch, bf16[512,2048]{1,0:T(8,128)(2,1)} %tokens.3, f32[1,2048]{1,0:T(1,128)} %bitcast.4), custom_call_target="tpu_custom_call" | custom-call | tf_op jit(solution)/shard_map/pallas_call | solution.py:651

commit v4 on v3

--- a/solution.py
+++ b/solution.py
@@ -418,9 +418,9 @@
             took(*slot(1, zz, 2 * k + 1, 2))
             core_out[b] = (acc[pl.ds(0, 2 * rows), lanes] + jnp.dot(
                 hid[theirs, late], down[b, late, :], preferred_element_type=f32)).astype(bf)
-            remote(part(core_out, i), part(core_in, i), 7, core_recv.at[i], next_core).start()
             keep[i % 3, :, lanes] = keep[i % 3, :, lanes] + jnp.dot(
                 hid[mine, late], down[b, late, :], preferred_element_type=f32)
+            remote(part(core_out, i), part(core_in, i), 7, core_recv.at[i], next_core).start()
 
         away = {"fs": jnp.where(core == 0, z, outer), "tp": jnp.where(core == 0, x_peer, t)}
 

time: 116 us -> 116 us (level)
  no operation moved by 1% of the time
where the time goes in v4:
time: 116 us
  Pallas kernels  116 us (100%)
    pallas_call x1, Pallas kernels, fused(): pl.pallas_call(kernel, out_shape=jax.ShapeDtypeStruct((pieces, rows, dc),...  112 us
    pallas_call x1, Pallas kernels, fused(): pl.pallas_call(closing, out_shape=jax.ShapeDtypeStruct((rows, width), bf)...  4.11 us

profile of v4, /device:TPU:0, one launch (start us, length us, event | category | flops | bytes accessed | tf_op | source)
XLA Modules:
  0.0 116.1 jit_solution(15439295417297880531)
XLA Ops:
  0.0 111.8 %shard_map.73.branch = bf16[16,512,128]{2,1,0:T(8,128)(2,1)} custom-call(bf16[512,2048]{1,0:T(8,128)(2,1)} %tokens.3, f32[512,2048]{1,0:T(8,128)} %up_in.1, f32[2048,512]{1,0:T(8,128)} %down_in.1, f32[1,2048]{1,0:T(1,128)} %bitcast.5, f32[1,512]{1,0:T(1,128)} %bitcast.7, f32[1,2048]{1,0:T(1,128)} %bitcast.6), custom_call_target="tpu_custom_call" | custom-call | tf_op jit(solution)/shard_map/pallas_call | solution.py:608
  111.8 4.1 %shard_map.74 = bf16[512,2048]{1,0:T(8,128)(2,1)} custom-call(bf16[16,512,128]{2,1,0:T(8,128)(2,1)} %shard_map.73.branch, bf16[512,2048]{1,0:T(8,128)(2,1)} %tokens.3, f32[1,2048]{1,0:T(1,128)} %bitcast.4), custom_call_target="tpu_custom_call" | custom-call | tf_op jit(solution)/shard_map/pallas_call | solution.py:651
